TPU v7x, 32 devices: a whole 2x2x4 slice. The times are simulated.
32 devices in a mesh: ep: 8 (over z, x), tp: 4 (over y, core).
Axes of the slice: x: 2, y: 2, z: 4, core: 2. Of those that a mesh axis runs over, the one named last changes fastest.
Arguments:
- x_mix: bfloat16 [2048, 2048], P('ep'), may hold values from -6 to 6
- mix_gain: float32 [2048], replicated, may hold values from 0.1 to 1.9
- w_query: bfloat16 [2048, 2048], P(None, 'tp'), may hold values from -0.125 to 0.125
- w_key: bfloat16 [2048, 2048], P(None, 'tp'), may hold values from -0.125 to 0.125
- w_value: bfloat16 [2048, 2048], P(None, 'tp'), may hold values from -0.125 to 0.125
- query_gain: float32 [64], replicated, may hold values from 1 to 1.8
- key_gain: float32 [64], replicated, may hold values from 1 to 1.8
- mix_lambda: float32 [16], P('tp'), may hold values from 0.3 to 0.8
- head_gain: float32 [128], replicated, may hold values from 0.1 to 1.9
- w_mix_out: bfloat16 [2048, 2048], P(None, 'tp'), may hold values from -0.125 to 0.125
- x_exp: bfloat16 [1024, 2048], P('ep'), may hold values from -6 to 6
- exp_gain: float32 [2048], replicated, may hold values from 0.1 to 1.9
- routes: int32 [1024, 4], P('ep'), may hold values from 0 to 7, all different within a row; in each aligned block of 128 rows (0 to 127, 128 to 255, ...) at most 96 rows name the same one
- route_weight: float32 [1024, 4], P('ep'), may hold values from 0.1 to 1
- w_gate: bfloat16 [8, 2048, 2048], P('ep', None, 'tp'), may hold values from -0.375 to 0.375
- w_up: bfloat16 [8, 2048, 2048], P('ep', None, 'tp'), may hold values from -0.375 to 0.375
- w_down: bfloat16 [8, 2048, 2048], P('ep', None, 'tp'), may hold values from -0.03125 to 0.03125
Outputs:
- attn_out: bfloat16 [2048, 2048], P('ep', 'tp')
- moe_out: bfloat16 [1024, 2048], P('ep', 'tp')
Inputs may be any that keep to these rules, and one draw needn't show every extreme that they name: `routes`: each row names 4 different experts. In each aligned block of 128 rows (the rows of one index of ep), no expert is named by more than 96 rows, a bound that some block reaches.
All inputs are finite; a program needn't handle non-finite values.
Results may differ from a plain program's by a relative error of at most 0.011.
Values may be sent and summed in bfloat16 or wider, within the bound.
A program may use at most 128 MiB of HBM per device.

v0:
```python
import jax
import jax.numpy as jnp
from jax import lax
from jax.sharding import PartitionSpec as P


def rms_rows(matrix, gain, epsilon):
    wide = matrix.astype(jnp.float32)
    return wide * lax.rsqrt(jnp.mean(wide * wide, axis=-1, keepdims=True) + epsilon) * gain


def slot_ids(chosen_rows, experts, capacity):
    flat_ids = chosen_rows.reshape(-1)
    onehot = (flat_ids[:, None] == lax.iota(jnp.int32, experts)[None, :]).astype(jnp.int32)
    before = jnp.cumsum(onehot, axis=0) - onehot
    position = jnp.sum(before * onehot, axis=1)
    return flat_ids * capacity + position


def attend(
    x_mix, mix_gain, w_query, w_key, w_value, query_gain, key_gain, mix_lambda, head_gain, w_mix_out
):
    row_count = x_mix.shape[0]
    head_size = query_gain.shape[0]
    head_count = w_query.shape[1] // (2 * head_size)
    normed = rms_rows(x_mix, mix_gain, 1e-05).astype(jnp.bfloat16)
    queries = jnp.dot(normed, w_query, preferred_element_type=jnp.float32).reshape(
        row_count, head_count, 2, head_size
    )
    queries = (rms_rows(queries, query_gain, 1e-06) * head_size ** (-0.5)).astype(jnp.bfloat16)
    key_rows = jnp.dot(normed, w_key, preferred_element_type=jnp.float32).reshape(
        row_count, head_count, 2, head_size
    )
    key_rows = (
        rms_rows(key_rows, key_gain, 1e-06)
        .astype(jnp.bfloat16)
        .reshape(row_count, head_count * 2 * head_size)
    )
    values = jnp.dot(normed, w_value, preferred_element_type=jnp.float32).astype(jnp.bfloat16)
    query_pos = lax.axis_index("ep") * row_count + lax.iota(jnp.int32, row_count)
    key_piece = lax.all_gather(key_rows, "ep", axis=0, tiled=True)
    value_piece = lax.all_gather(values, "ep", axis=0, tiled=True)
    piece_rows = key_piece.shape[0]
    key_piece = key_piece.reshape(piece_rows, head_count, 2, head_size)
    value_piece = value_piece.reshape(piece_rows, head_count, 2 * head_size)
    scores = jnp.einsum("qhcd,khcd->cqhk", queries, key_piece, preferred_element_type=jnp.float32)
    key_pos = lax.iota(jnp.int32, piece_rows)
    visible = key_pos[None, :] <= query_pos[:, None]
    weights_exp = jnp.where(visible[None, :, None, :], jnp.exp(scores), 0.0)
    denominator = jnp.sum(weights_exp, axis=-1)
    numerator = jnp.einsum(
        "cqhk,khd->cqhd",
        weights_exp.astype(jnp.bfloat16),
        value_piece,
        preferred_element_type=jnp.float32,
    )
    numerator, denominator = (numerator, denominator)
    head_mix = (
        numerator[0] / denominator[0][..., None]
        - mix_lambda[None, :, None] * numerator[1] / denominator[1][..., None]
    )
    head_rows = (rms_rows(head_mix, head_gain, 1e-05) * 0.8).astype(jnp.bfloat16)
    head_rows = head_rows.reshape(row_count, head_count * 2 * head_size)
    projected = jnp.dot(
        lax.all_gather(head_rows, "tp", axis=1, tiled=True),
        w_mix_out,
        preferred_element_type=jnp.float32,
    )
    return projected.astype(jnp.bfloat16)


def route_experts(x_exp, exp_gain, routes, route_weight, w_gate, w_up, w_down):
    row_count = x_exp.shape[0]
    top_count = routes.shape[1]
    model_width = x_exp.shape[1]
    experts = lax.axis_size("ep")
    capacity = 3 * row_count * top_count // (2 * experts)
    gate_local = w_gate[0]
    up_local = w_up[0]
    down_local = w_down[0]
    local_width = down_local.shape[1]
    normed = rms_rows(x_exp, exp_gain, 1e-05).astype(jnp.bfloat16)
    slot_index = slot_ids(routes, experts, capacity)
    pair_rows = lax.iota(jnp.int32, row_count * top_count) // top_count
    source = jnp.zeros((experts * capacity,), jnp.int32).at[slot_index].set(pair_rows)
    filled = jnp.zeros((experts * capacity,), jnp.bool_).at[slot_index].set(True)
    picked_rows = jnp.where(filled[:, None], normed[source], jnp.zeros((), jnp.bfloat16))
    outgoing = picked_rows.reshape(experts, capacity, model_width)
    incoming = lax.all_to_all(outgoing, "ep", split_axis=0, concat_axis=0, tiled=True)
    item_count = incoming.shape[1]
    flat_rows = incoming.reshape(-1, model_width)
    gate_pre = jnp.dot(flat_rows, gate_local, preferred_element_type=jnp.float32)
    up_pre = jnp.dot(flat_rows, up_local, preferred_element_type=jnp.float32)
    expert_gate_pre = gate_pre
    expert_up_pre = up_pre
    expert_gate_pre = jnp.minimum(expert_gate_pre, 7.0)
    expert_up_pre = jnp.clip(expert_up_pre, -7.0, 7.0)
    hidden = (
        expert_gate_pre * jax.nn.sigmoid(1.702 * expert_gate_pre) * (expert_up_pre + 1.0)
    ).astype(jnp.bfloat16)
    result = jnp.dot(
        lax.all_gather(hidden, "tp", axis=1, tiled=True),
        down_local,
        preferred_element_type=jnp.float32,
    )
    result = result.astype(jnp.bfloat16).reshape(experts, item_count, local_width)
    returned = lax.all_to_all(result, "ep", split_axis=0, concat_axis=0, tiled=True)
    picked = returned.reshape(experts * capacity, local_width)[slot_index]
    picked = picked.reshape(row_count, top_count, local_width).astype(jnp.float32)
    combined = jnp.sum(picked * route_weight[:, :, None], axis=1)
    return combined.astype(jnp.bfloat16)


def body(
    x_mix,
    mix_gain,
    w_query,
    w_key,
    w_value,
    query_gain,
    key_gain,
    mix_lambda,
    head_gain,
    w_mix_out,
    x_exp,
    exp_gain,
    routes,
    route_weight,
    w_gate,
    w_up,
    w_down,
):
    attn_out = attend(
        x_mix,
        mix_gain,
        w_query,
        w_key,
        w_value,
        query_gain,
        key_gain,
        mix_lambda,
        head_gain,
        w_mix_out,
    )
    moe_out = route_experts(x_exp, exp_gain, routes, route_weight, w_gate, w_up, w_down)
    return (attn_out, moe_out)


def solution(mesh):
    return jax.shard_map(
        body,
        mesh=mesh,
        in_specs=(
            P("ep", None),
            P(),
            P(None, "tp"),
            P(None, "tp"),
            P(None, "tp"),
            P(),
            P(),
            P("tp"),
            P(),
            P(None, "tp"),
            P("ep", None),
            P(),
            P("ep", None),
            P("ep", None),
            P("ep", None, "tp"),
            P("ep", None, "tp"),
            P("ep", None, "tp"),
        ),
        out_specs=(P("ep", "tp"), P("ep", "tp")),
        check_vma=False,
    )
```

profile of v0, /device:TPU:0, one launch (start us, length us, event | category | flops | bytes accessed | tf_op | source)
XLA Modules:
  0.0 233.7 jit_solution(14530396072772306226)
XLA Ops:
  7.2 0.0 copy-start
  7.2 0.0 all-gather.7.cloned.1.call-start
  7.2 1.6 fusion.4
  8.9 3.5 %fusion.52 = (f32[256,512]{1,0:T(8,128)S(1)}, f32[256,512]{1,0:T(8,128)}) fusion(bf16[2048,512]{1,0:T(8,128)(2,1)} %param.20, bf16[256,2048]{1,0:T(8,128)(2,1)} %param.17, f32[2048]{0:T(1024)} %param.18, f32[256]{0:T(256)S(1)} %add_rsqrt_fusion.3), kind=kOutput, calls=%fused_computation.90 | convolution fusion | flops 539099136 | bytes 4203520 | tf_op jit(solution)/shard_map/dot_general | solution.py:31
  12.4 0.2 copy.26
  12.6 0.0 copy-start.5
  12.6 0.0 copy-start.2
  12.6 0.1 bitcast_reduce_fusion
  12.7 0.9 mul.194
  13.5 1.2 copy.27
  14.8 0.1 mul.198
  14.9 1.9 multiply_convert_fusion.2
  16.7 0.0 all-gather.7.cloned.1.call-update
  16.8 0.1 copy.36
  16.9 0.1 eq.29
  17.0 0.1 eq.25
  17.1 1.1 reduce-window.6
  18.3 0.2 slice_reduce_fusion
  18.5 0.1 copy.35
  18.7 0.1 mul.226
  18.8 0.1 fusion.37
  18.9 2.4 %scatter_custom_fusion.1 = s32[768]{0:T(1024)S(1)} fusion(s32[512]{0:T(512)S(1)} %bitcast.123, s32[512]{0:T(512)S(1)} %add_select_fusion, s32[]{:T(128)} %constant.65.clone.1), kind=kCustom, calls=%fused_computation.76 | custom fusion | bytes 3076 | tf_op jit(solution)/shard_map/scatter | solution.py:85
  21.4 0.2 fusion.23
  21.6 2.4 %scatter_custom_fusion = pred[768]{0:T(1024)(128)(4,1)S(1)} fusion(s32[512]{0:T(512)S(1)} %bitcast.124, pred[512]{0:T(512)(128)(4,1)S(1)} %broadcast.164, pred[]{:T(512)} %constant.25.clone.1), kind=kCustom, calls=%fused_computation.79 | custom fusion | bytes 769 | tf_op jit(solution)/shard_map/scatter | solution.py:86
  24.0 0.1 broadcast_in_dim.32
  24.1 0.2 fusion.25
  24.3 4.3 %gather_fusion = bf16[768,2048]{1,0:T(8,128)(2,1)} fusion(bf16[128,2048]{1,0:T(8,128)(2,1)S(1)} %fusion.25, s32[1024]{0:T(1024)S(1)} %pad_clamp_fusion.1), kind=kCustom, calls=%fused_computation | custom fusion | bytes 6294528 | tf_op jit(solution)/shard_map/gather | solution.py:87
  28.6 3.9 %broadcast_select_fusion = bf16[8,96,2048]{2,1,0:T(8,128)(2,1)} fusion(bf16[8,96,2048]{2,1,0:T(8,128)(2,1)} %bitcast.118, pred[8,96]{1,0:T(8,128)(4,1)S(1)} %broadcast_in_dim.32), kind=kLoop, calls=%fused_computation.9 | loop fusion | flops 1572864 | bytes 6292224 | tf_op jit(solution)/shard_map/jit(_where)/select_n | solution.py:87
  32.5 7.4 %all-to-all-start = ((bf16[8,96,2048]{2,1,0:T(8,128)(2,1)}), bf16[8,96,2048]{2,1,0:T(8,128)(2,1)}, u32[]{:S(2)}, u32[]{:S(2)}) async-start(bf16[8,96,2048]{2,1,0:T(8,128)(2,1)} %broadcast_select_fusion), calls=%async_computation | async-start | bytes 6291456 | tf_op jit(solution)/shard_map/all_to_all | solution.py:89
  39.9 0.0 all-gather.5.cloned.1.call-start
  40.0 3.0 %convolution_convert_fusion.1 = bf16[256,512]{1,0:T(8,128)(2,1)} fusion(bf16[2048,512]{1,0:T(8,128)(2,1)} %param.21, bf16[256,2048]{1,0:T(8,128)(2,1)S(1)} %copy-done.3, f32[2048]{0:T(1024)S(1)} %copy-done.11, f32[256]{0:T(256)S(1)} %add_rsqrt_fusion.3), kind=kOutput, calls=%fused_computation.30 | convolution fusion | flops 539099136 | bytes 3417088 | tf_op jit(solution)/shard_map/dot_general | solution.py:39
  43.1 0.0 all-gather.5.cloned.1.call-update
  43.1 0.0 all-gather.11.cloned.1.call-start
  43.1 93.0 %all-to-all-done = bf16[8,96,2048]{2,1,0:T(8,128)(2,1)} async-done(((bf16[8,96,2048]{2,1,0:T(8,128)(2,1)}), bf16[8,96,2048]{2,1,0:T(8,128)(2,1)}, u32[]{:S(2)}, u32[]{:S(2)}) %all-to-all-start) | async-done | bytes 3145760 | tf_op jit(solution)/shard_map/all_to_all | solution.py:89
  136.1 3.8 %fusion.11 = f32[768,512]{1,0:T(8,128)S(1)} fusion(bf16[768,2048]{1,0:T(8,128)(2,1)} %bitcast.25, bf16[1,2048,512]{2,1,0:T(8,128)(2,1)S(1)} %copy-done), kind=kOutput, calls=%fused_computation.19 | convolution fusion | flops 1610612736 | bytes 6815744 | tf_op jit(solution)/shard_map/dot_general | solution.py:92
  140.0 0.0 copy-start.6
  140.0 0.0 copy-start.9
  140.0 4.9 %multiply_convert_fusion = bf16[768,512]{1,0:T(8,128)(2,1)} fusion(f32[768,512]{1,0:T(8,128)S(1)} %fusion.11, bf16[768,2048]{1,0:T(8,128)(2,1)} %bitcast.25, bf16[1,2048,512]{2,1,0:T(8,128)(2,1)S(1)} %copy-done.10), kind=kOutput, calls=%fused_computation.24 | convolution fusion | flops 1614544896 | bytes 7602176 | tf_op jit(solution)/shard_map/dot_general | solution.py:93
  144.9 0.0 all-gather.11.cloned.1.call-update
  144.9 0.2 all-gather.9.cloned.1.call-start
  145.2 0.1 broadcast_bitcast_fusion
  145.3 3.5 %multiply_reduce_fusion.1 = (f32[256,4,2]{0,2,1:T(2,128)S(1)}, f32[256,512]{0,1:T(8,128)}) fusion(bf16[2048,512]{1,0:T(8,128)(2,1)} %param.19, bf16[256,2048]{1,0:T(8,128)(2,1)S(1)} %copy-done.3, f32[2048]{0:T(1024)S(1)} %copy-done.11, f32[256]{0:T(256)S(1)} %add_rsqrt_fusion.3), kind=kOutput, calls=%fused_computation.49 | convolution fusion | flops 539228160 | bytes 3687424 | tf_op jit(solution)/shard_map/dot_general | solution.py:27
  148.8 0.3 iota_compare_fusion
  149.1 0.0 all-gather.7.cloned.1.call-done
  149.1 4.0 %copy.28 = bf16[2048,512]{0,1:T(8,128)(2,1)} copy(bf16[2048,512]{1,0:T(8,128)(2,1)} %all-gather.7.cloned.1.call-done) | data formatting | bytes 4194304 | tf_op jit(solution)/shard_map/all_gather | solution.py:41
  153.1 8.7 %all-gather.5.cloned.1.call-done = bf16[2048,512]{1,0:T(8,128)(2,1)} async-done(((bf16[256,512]{1,0:T(8,128)(2,1)}), bf16[2048,512]{1,0:T(8,128)(2,1)}) %all-gather.5.cloned.1.call-update) | async-done | bytes 2097168 | tf_op jit(solution)/shard_map/all_gather | solution.py:42
  161.9 3.9 %copy.42 = bf16[2048,512]{0,1:T(8,128)(2,1)} copy(bf16[2048,512]{1,0:T(8,128)(2,1)} %all-gather.5.cloned.1.call-done) | data formatting | bytes 4194304 | tf_op jit(solution)/shard_map/reshape | solution.py:45
  165.8 6.7 %fusion = (f32[2,256,4]{1,2,0:T(4,128)S(1)}, bf16[2,256,4,2048]{1,3,2,0:T(8,128)(2,1)S(1)}) fusion(pred[256,2048]{0,1:T(8,128)(4,1)S(1)} %iota_compare_fusion, bf16[2048,4,2,64]{0,3,2,1:T(8,128)(2,1)} %bitcast.120, f32[64]{0:T(128)S(1)} %copy-done.12, f32[256,4,2]{0,2,1:T(2,128)S(1)} %add_rsqrt_fusion, f32[256,512]{0,1:T(8,128)S(1)} %copy-done.13), kind=kOutput, calls=%fused_computation.5 | convolution fusion | flops 549976064 | bytes 11550976 | tf_op jit(solution)/shard_map/qhcd,khcd->cqhk/dot_general | solution.py:46
  172.5 1.3 fusion.20
  173.8 0.2 fusion.34
  174.0 0.1 fusion.51
  174.1 0.9 fusion.33
  175.0 0.0 all-gather.9.cloned.1.call-update
  175.0 0.0 copy-start.7
  175.1 15.4 %all-gather.11.cloned.1.call-done = bf16[768,2048]{1,0:T(8,128)(2,1)} async-done(((bf16[768,512]{1,0:T(8,128)(2,1)}), bf16[768,2048]{1,0:T(8,128)(2,1)}) %all-gather.11.cloned.1.call-update) | async-done | bytes 3145744 | tf_op jit(solution)/shard_map/all_gather | solution.py:102
  190.5 5.2 %fusion.17 = bf16[768,512]{1,0:T(8,128)(2,1)} fusion(bf16[768,2048]{1,0:T(8,128)(2,1)} %all-gather.11.cloned.1.call-done, bf16[1,2048,512]{2,1,0:T(8,128)(2,1)} %param.33), kind=kOutput, calls=%fused_computation.25 | convolution fusion | flops 1611005952 | bytes 6029312 | tf_op jit(solution)/shard_map/dot_general | solution.py:101
  195.7 5.5 %all-to-all-start.1 = ((bf16[8,96,512]{2,1,0:T(8,128)(2,1)}), bf16[8,96,512]{2,1,0:T(8,128)(2,1)S(1)}, u32[]{:S(2)}, u32[]{:S(2)}) async-start(bf16[8,96,512]{2,1,0:T(8,128)(2,1)} %bitcast.122), calls=%async_computation.1 | async-start | bytes 1572864 | tf_op jit(solution)/shard_map/all_to_all | solution.py:107
  201.2 0.1 copy.38
  201.4 7.9 %all-gather.9.cloned.1.call-done = bf16[256,2048]{0,1:T(8,128)(2,1)} async-done(((bf16[256,512]{0,1:T(8,128)(2,1)}), bf16[256,2048]{0,1:T(8,128)(2,1)}) %all-gather.9.cloned.1.call-update) | async-done | bytes 1048592 | tf_op jit(solution)/shard_map/all_gather | solution.py:65
  209.2 3.3 %convolution_convert_fusion = bf16[256,512]{1,0:T(8,128)(2,1)} fusion(bf16[256,2048]{0,1:T(8,128)(2,1)} %all-gather.9.cloned.1.call-done, bf16[2048,512]{1,0:T(8,128)(2,1)} %param.26), kind=kOutput, calls=%fused_computation.29 | convolution fusion | flops 537001984 | bytes 3407872 | tf_op jit(solution)/shard_map/dot_general | solution.py:64
  212.6 9.2 %all-to-all-done.1 = bf16[8,96,512]{2,1,0:T(8,128)(2,1)S(1)} async-done(((bf16[8,96,512]{2,1,0:T(8,128)(2,1)}), bf16[8,96,512]{2,1,0:T(8,128)(2,1)S(1)}, u32[]{:S(2)}, u32[]{:S(2)}) %all-to-all-start.1) | async-done | bytes 786464 | tf_op jit(solution)/shard_map/all_to_all | solution.py:107
  221.8 2.6 %gather_fusion.1 = bf16[512,512]{1,0:T(8,128)(2,1)} fusion(bf16[768,512]{1,0:T(8,128)(2,1)S(1)} %bitcast.117, s32[1024]{0:T(1024)S(1)} %pad_clamp_fusion), kind=kCustom, calls=%fused_computation.1 | custom fusion | bytes 1050624 | tf_op jit(solution)/shard_map/gather | solution.py:108
  224.4 1.4 reshape.170
  225.8 1.4 multiply_reduce_fusion
  (40 shorter events, 0.2 us)
Async XLA Ops:
  7.2 129.0 %copy-start = (bf16[1,2048,512]{2,1,0:T(8,128)(2,1)S(1)}, bf16[1,2048,512]{2,1,0:T(8,128)(2,1)}, u32[]{:S(2)}) copy-start(bf16[1,2048,512]{2,1,0:T(8,128)(2,1)} %param.31) | copy-start | bytes 6291460
  7.2 141.9 %all-gather.7.cloned.1.call-start = ((), (), s32[]{:S(2)}) async-start(), calls=%async_computation.3 | async-start | bytes 2359296 | tf_op jit(solution)/shard_map/all_gather | solution.py:41
  12.4 2.4 %copy-start.8 = (f32[64]{0:T(128)S(1)}, f32[64]{0:T(128)}, u32[]{:S(2)}) copy-start(f32[64]{0:T(128)} %param.23) | copy-start | bytes 772
  12.6 4.2 %copy-start.5 = (s32[128,4]{0,1:T(4,128)S(1)}, s32[128,4]{0,1:T(4,128)}, u32[]{:S(2)}) copy-start(s32[128,4]{0,1:T(4,128)} %param.29) | copy-start | bytes 6148
  12.6 8.8 %copy-start.2 = (bf16[128,2048]{1,0:T(8,128)(2,1)S(1)}, bf16[128,2048]{1,0:T(8,128)(2,1)}, u32[]{:S(2)}) copy-start(bf16[128,2048]{1,0:T(8,128)(2,1)} %param.27) | copy-start | bytes 1572868
  12.7 11.5 %copy-start.4 = (f32[2048]{0:T(1024)S(1)}, f32[2048]{0:T(1024)}, u32[]{:S(2)}) copy-start(f32[2048]{0:T(1024)} %param.28) | copy-start | bytes 24580
  32.5 7.5 %copy-start.3 = (bf16[256,2048]{1,0:T(8,128)(2,1)S(1)}, bf16[256,2048]{1,0:T(8,128)(2,1)}, u32[]{:S(2)}) copy-start(bf16[256,2048]{1,0:T(8,128)(2,1)} %param.17) | copy-start | bytes 3145732
  32.5 7.5 %copy-start.11 = (f32[2048]{0:T(1024)S(1)}, f32[2048]{0:T(1024)}, u32[]{:S(2)}) copy-start(f32[2048]{0:T(1024)} %param.18) | copy-start | bytes 24580
  32.5 103.6 %all-to-all-start = ((bf16[8,96,2048]{2,1,0:T(8,128)(2,1)}), bf16[8,96,2048]{2,1,0:T(8,128)(2,1)}, u32[]{:S(2)}, u32[]{:S(2)}) async-start(bf16[8,96,2048]{2,1,0:T(8,128)(2,1)} %broadcast_select_fusion), calls=%async_computation | async-start | bytes 6291456 | tf_op jit(solution)/shard_map/all_to_all | solution.py:89
  39.9 121.9 %all-gather.5.cloned.1.call-start = ((), (), s32[]{:S(2)}) async-start(), calls=%async_computation.2 | async-start | bytes 2359296 | tf_op jit(solution)/shard_map/all_gather | solution.py:42
  43.1 147.4 %all-gather.11.cloned.1.call-start = ((), (), s32[]{:S(2)}) async-start(), calls=%async_computation.5 | async-start | bytes 3932160 | tf_op jit(solution)/shard_map/all_gather | solution.py:102
  136.1 3.8 %copy-start.10 = (bf16[1,2048,512]{2,1,0:T(8,128)(2,1)S(1)}, bf16[1,2048,512]{2,1,0:T(8,128)(2,1)}, u32[]{:S(2)}) copy-start(bf16[1,2048,512]{2,1,0:T(8,128)(2,1)} %param.32) | copy-start | bytes 6291460
  140.0 5.2 %copy-start.6 = (f32[4]{0:T(128)S(1)}, f32[4]{0:T(128)}, u32[]{:S(2)}) copy-start(f32[4]{0:T(128)} %param.24) | copy-start | bytes 52
  140.0 5.2 %copy-start.9 = (f32[128]{0:T(128)S(1)}, f32[128]{0:T(128)}, u32[]{:S(2)}) copy-start(f32[128]{0:T(128)} %param.25) | copy-start | bytes 1540
  144.9 64.3 %all-gather.9.cloned.1.call-start = ((), (), s32[]{:S(2)}) async-start(), calls=%async_computation.4 | async-start | bytes 1310720 | tf_op jit(solution)/shard_map/all_gather | solution.py:65
  153.1 12.7 %copy-start.12 = (f32[64]{0:T(128)S(1)}, f32[64]{0:T(128)}, u32[]{:S(2)}) copy-start(f32[64]{0:T(128)} %param.22) | copy-start | bytes 772
  153.1 12.7 %copy-start.13 = (f32[256,512]{0,1:T(8,128)S(1)}, f32[256,512]{0,1:T(8,128)}, u32[]{:S(2)}) copy-start(f32[256,512]{0,1:T(8,128)} %get-tuple-element.11) | copy-start | bytes 1572868
  165.8 6.7 %copy-start.1 = (bf16[2048,512]{0,1:T(8,128)(2,1)S(1)}, bf16[2048,512]{0,1:T(8,128)(2,1)}, u32[]{:S(2)}) copy-start(bf16[2048,512]{0,1:T(8,128)(2,1)} %copy.42) | copy-start | bytes 6291460
  175.0 26.2 %copy-start.7 = (f32[128,4]{0,1:T(4,128)S(1)}, f32[128,4]{0,1:T(4,128)}, u32[]{:S(2)}) copy-start(f32[128,4]{0,1:T(4,128)} %param.30) | copy-start | bytes 6148
  195.7 26.1 %all-to-all-start.1 = ((bf16[8,96,512]{2,1,0:T(8,128)(2,1)}), bf16[8,96,512]{2,1,0:T(8,128)(2,1)S(1)}, u32[]{:S(2)}, u32[]{:S(2)}) async-start(bf16[8,96,512]{2,1,0:T(8,128)(2,1)} %bitcast.122), calls=%async_computation.1 | async-start | bytes 1572864 | tf_op jit(solution)/shard_map/all_to_all | solution.py:107
Sparse Core Ops, SparseCore 0:
  16.9 67.8 all-gather.6
  87.5 74.3 all-gather.4
  163.4 27.0 all-gather.10
  192.5 16.6 all-gather.8
where the time goes:
time: 234 us
  waiting for transfers between devices  134 us (57%)
  matrix products  35.2 us (15%)
  local copies, waits for them, and re-layouts  24.7 us (11%)
  between operations  14.1 us (6%)
  starting transfers between devices  13.3 us (6%)
  other arithmetic  12 us (5%)
    all_to_all x1, waiting for transfers between devices, route_experts(): lax.all_to_all(outgoing, 'ep', split_axis=0, concat_axis=0, tiled=True)  93 us
    all_gather x1, waiting for transfers between devices, route_experts(): lax.all_gather(hidden, 'tp', axis=1, tiled=True)  15.4 us
    all_to_all x1, waiting for transfers between devices, route_experts(): lax.all_to_all(result, 'ep', split_axis=0, concat_axis=0, tiled=True)  9.19 us
    all_gather x1, waiting for transfers between devices, attend(): value_piece = lax.all_gather(values, 'ep', axis=0, tiled=True)  8.72 us
    all_gather x1, waiting for transfers between devices, attend(): lax.all_gather(head_rows, 'tp', axis=1, tiled=True)  7.88 us
    all_to_all x1, starting transfers between devices, route_experts(): lax.all_to_all(outgoing, 'ep', split_axis=0, concat_axis=0, tiled=True)  7.43 us
    dot_general x1, matrix products, attend(): jnp.einsum('qhcd,khcd->cqhk', queries, key_piece, preferred_element_type=...  6.69 us
    all_to_all x1, starting transfers between devices, route_experts(): lax.all_to_all(result, 'ep', split_axis=0, concat_axis=0, tiled=True)  5.51 us
  transfers between devices with their start and end apart: 6, of which 5 were waited for; matrix products, arithmetic and copies ran while one was open for 24% of the time, Pallas kernels for 0%

commit v1 on v0

v1 whole, which is shorter than its diff:
```python
import functools
import jax
import jax.numpy as jnp
from jax import lax
from jax.experimental import pallas as pl
from jax.experimental.pallas import tpu as pltpu
from jax.sharding import PartitionSpec as P


def rms_rows(matrix, gain, epsilon):
    wide = matrix.astype(jnp.float32)
    return wide * lax.rsqrt(jnp.mean(wide * wide, axis=-1, keepdims=True) + epsilon) * gain


def kernel(
    n,
    parts,
    top,
    cap,
    head_size,
    q_ref,
    kv_ref,
    tok_ref,
    info_ref,
    lam_ref,
    hgain_ref,
    wout_ref,
    wgate_ref,
    wup_ref,
    wdown_ref,
    attn_ref,
    moe_ref,
    kv,
    tok,
    info,
    flat,
    hid,
    res,
    ret,
    numer,
    denom,
    heads,
    tok_s,
    tok_r,
    info_s,
    info_r,
    core_s,
    core_r,
    kv_s,
    kv_r,
    hid_s,
    hid_r,
    ret_s,
    ret_r,
    head_s,
    head_r,
):
    half = n // 2
    me = lax.axis_index("ep")
    mine = lax.axis_index("tp")
    odd = me % 2
    pos = (1 - odd) * (me // 2) + odd * (n - 1 - me // 2)

    def at(place):
        place = (place + 2 * n) % n
        high = place // half
        return (1 - high) * 2 * place + high * (2 * (n - 1 - place) + 1)

    right, left = at(pos + 1), at(pos - 1)
    core = mine % 2
    twin = mine + 1 - 2 * core
    rows_b, model = tok_ref.shape
    rows_a, pair_width = kv_ref.shape
    width = pair_width // 2
    side = model // 2
    local = wgate_ref.shape[1]
    f32, bf16 = jnp.float32, jnp.bfloat16

    barrier = pltpu.get_barrier_semaphore()
    for i in range(1, n):
        pl.semaphore_signal(
            barrier, inc=1, device_id={"ep": (me + i) % n}, device_id_type=pl.DeviceIdType.MESH
        )
    for i in range(1, parts):
        pl.semaphore_signal(
            barrier, inc=1, device_id={"tp": (mine + i) % parts}, device_id_type=pl.DeviceIdType.MESH
        )
    pl.semaphore_wait(barrier, n - 1 + parts - 1)

    def push(src, dst, s_sem, r_sem, where):
        return pltpu.make_async_remote_copy(
            src_ref=src,
            dst_ref=dst,
            send_sem=s_sem,
            recv_sem=r_sem,
            device_id=where,
            device_id_type=pl.DeviceIdType.MESH,
        )

    def span(step, way, rows):
        if step < half:
            return pl.ds(0, rows)
        return pl.ds(way * (rows // 2), rows // 2)

    def held(step, way):
        return at(pos - step) if way == 0 else at(pos + step)

    def tok_copies(step):
        out = []
        for way in (0, 1):
            where = {"ep": right if way == 0 else left}
            b = held(step - 1, way)
            cols = pl.ds(pl.multiple_of(core * side, side), side)
            rows = span(step, way, rows_b)
            if step == 1:
                src = tok_ref.at[rows, cols]
            else:
                src = tok.at[b, rows, cols]
            i = 2 * (step - 1) + way
            out.append(push(src, tok.at[b, rows, cols], tok_s.at[i], tok_r.at[i], where))
            if step < half or way == 0:
                src = info_ref if step == 1 else info.at[b]
                out.append(push(src, info.at[b], info_s.at[i], info_r.at[i], where))
        return out

    def kv_copies(step):
        out = []
        for way in (0, 1):
            where = {"ep": right if way == 0 else left}
            b = held(step - 1, way)
            rows = span(step, way, rows_a)
            src = kv_ref.at[rows] if step == 1 else kv.at[b, rows]
            i = 2 * (step - 1) + way
            out.append(push(src, kv.at[b, rows], kv_s.at[i], kv_r.at[i], where))
        return out

    def core_copies(step):
        out = []
        for way in (0, 1):
            b = held(step, way)
            cols = pl.ds(pl.multiple_of(core * side, side), side)
            ref = tok.at[b, span(step, way, rows_b), cols]
            i = 2 * (step - 1) + way
            out.append(push(ref, ref, core_s.at[i], core_r.at[i], {"tp": twin}))
        return out

    def start(copies):
        for copy in copies:
            copy.start()
        return copies

    def wait_recv(copies):
        for copy in copies:
            copy.wait_recv()

    def slot_block(slot):
        return held((slot + 1) // 2, (slot + 1) % 2)

    def slot_rows(block_info, expert):
        named = block_info[:top, :] == expert
        member = jnp.sum(named.astype(f32), axis=0, keepdims=True)
        row = lax.broadcasted_iota(jnp.int32, (rows_b, rows_b), 0)
        col = lax.broadcasted_iota(jnp.int32, (rows_b, rows_b), 1)
        earlier = (row < col).astype(bf16)
        spread = jnp.broadcast_to(member, (16, rows_b)).astype(bf16)
        before = jnp.dot(spread, earlier, preferred_element_type=f32)[:1]
        place = lax.broadcasted_iota(jnp.int32, (cap, rows_b), 0).astype(f32)
        return ((place == before) & (member > 0.0)).astype(f32).astype(bf16), named

    def compact(slot):
        if slot == 0:
            rows, notes = tok_ref[...], info_ref[...]
        else:
            b = slot_block(slot)
            rows, notes = tok[b], info[b]
        chosen, _ = slot_rows(notes, me.astype(f32))
        flat[slot * cap : (slot + 1) * cap, :] = jnp.dot(
            chosen, rows, preferred_element_type=f32
        ).astype(bf16)

    groups = 4
    per = n // groups
    size = per * cap
    tile = min(256, local)

    def hidden_group(g):
        for slot in range(g * per, (g + 1) * per):
            compact(slot)

        @pl.loop(0, local // tile)
        def _(c):
            cols = pl.ds(pl.multiple_of(c * tile, tile), tile)
            rows = flat[g * size : (g + 1) * size, :]
            gate = jnp.dot(rows, wgate_ref[:, cols], preferred_element_type=f32)
            up = jnp.dot(rows, wup_ref[:, cols], preferred_element_type=f32)
            gate = jnp.minimum(gate, 7.0)
            up = jnp.clip(up, -7.0, 7.0)
            value = gate * jax.nn.sigmoid(1.702 * gate) * (up + 1.0)
            hid[mine, g * size : (g + 1) * size, cols] = value.astype(bf16)

        out = []
        for i in range(1, parts):
            ref = hid.at[mine, pl.ds(g * size, size)]
            k = g * parts + i
            out.append(push(ref, ref, hid_s.at[k], hid_r.at[k], {"tp": (mine + i) % parts}))
        return start(out)

    def attend(k_of, diagonal):
        @pl.loop(0, width // (2 * head_size))
        def _(h):
            cols = pl.ds(pl.multiple_of(h * 2 * head_size, 2 * head_size), 2 * head_size)
            vcols = pl.ds(pl.multiple_of(width + h * 2 * head_size, 2 * head_size), 2 * head_size)
            query, key, value = q_ref[:, cols], k_of(cols), k_of(vcols)
            for c in (0, 1):
                part = slice(c * head_size, (c + 1) * head_size)
                scores = lax.dot_general(
                    query[:, part],
                    key[:, part],
                    (((1,), (1,)), ((), ())),
                    preferred_element_type=f32,
                )
                expo = jnp.exp(scores)
                if diagonal:
                    row = lax.broadcasted_iota(jnp.int32, expo.shape, 0)
                    col = lax.broadcasted_iota(jnp.int32, expo.shape, 1)
                    expo = jnp.where(col <= row, expo, 0.0)
                total = jnp.broadcast_to(
                    jnp.sum(expo, axis=1, keepdims=True), (rows_a, 128)
                )
                mixed = jnp.dot(expo.astype(bf16), value, preferred_element_type=f32)
                if diagonal:
                    numer[c, :, cols] = mixed
                    denom[c, h] = total
                else:
                    numer[c, :, cols] += mixed
                    denom[c, h] += total

    def attend_step(step):
        for way in (0, 1) if step < half else (0,):
            b = held(step, way)

            @pl.when(b < me)
            def _():
                attend(lambda cols: kv[b, :, cols], False)

    sent = []
    now = start(tok_copies(1))
    sent += now
    attend(lambda cols: kv_ref[:, cols], True)
    cores, hids, kv_now = [], [], None
    early = max(1, half - 1)
    for step in range(1, half + 1):
        wait_recv(now)
        if step < half:
            now = start(tok_copies(step + 1))
            sent += now
        if step == early:
            kv_now = start(kv_copies(1))
            sent += kv_now
        cores = start(core_copies(step))
        sent += cores
        wait_recv(cores)
        for g in range(groups):
            if (g * per + per) // 2 == step:
                hids += hidden_group(g)
    sent += hids

    moe_step = (half + 1) // 2
    for step in range(1, half + 1):
        wait_recv(kv_now)
        if step < half:
            kv_now = start(kv_copies(step + 1))
            sent += kv_now
        attend_step(step)
        if step == moe_step:
            wait_recv(hids)

            @pl.loop(0, groups)
            def _(g):
                rows = pl.ds(pl.multiple_of(g * size, size), size)
                total = jnp.zeros((size, moe_ref.shape[1]), f32)
                for t in range(parts):
                    total += jnp.dot(
                        hid[t, rows, :],
                        wdown_ref[t * local : (t + 1) * local, :],
                        preferred_element_type=f32,
                    )
                res[rows, :] = total.astype(bf16)

            ret[me] = res[0:cap, :]
            rets = []
            for slot in range(1, n):
                b = slot_block(slot)
                d = (slot + 1) // 2 if slot % 2 == 1 else n - slot // 2
                rets.append(
                    push(
                        res.at[pl.ds(slot * cap, cap)],
                        ret.at[me],
                        ret_s.at[d],
                        ret_r.at[d],
                        {"ep": b},
                    )
                )
            sent += start(rets)

    @pl.loop(0, width // (2 * head_size))
    def _(h):
        cols = pl.ds(pl.multiple_of(h * 2 * head_size, 2 * head_size), 2 * head_size)
        first = numer[0, :, cols] / denom[0, h][:, :1]
        second = numer[1, :, cols] / denom[1, h][:, :1]
        mix = first - lam_ref[h] * second
        heads[mine, :, cols] = (rms_rows(mix, hgain_ref[...], 1e-05) * 0.8).astype(bf16)

    outs = []
    for i in range(1, parts):
        ref = heads.at[mine]
        outs.append(push(ref, ref, head_s.at[i], head_r.at[i], {"tp": (mine + i) % parts}))
    sent += start(outs)

    wait_recv(rets)
    total = jnp.zeros(moe_ref.shape, f32)
    notes = info_ref[...]
    for e in range(n):
        chosen, named = slot_rows(notes, float(e))
        weight = jnp.sum(jnp.where(named, notes[top:, :], 0.0), axis=0, keepdims=True)
        picked = lax.dot_general(
            chosen, ret[e], (((0,), (0,)), ((), ())), preferred_element_type=f32
        )
        total += picked * weight.T
    moe_ref[...] = total.astype(bf16)

    wait_recv(outs)
    result = jnp.zeros(attn_ref.shape, f32)
    for t in range(parts):
        result += jnp.dot(
            heads[t], wout_ref[t * width : (t + 1) * width, :], preferred_element_type=f32
        )
    attn_ref[...] = result.astype(bf16)
    for copy in sent:
        copy.wait_send()


def body(
    x_mix,
    mix_gain,
    w_query,
    w_key,
    w_value,
    query_gain,
    key_gain,
    mix_lambda,
    head_gain,
    w_mix_out,
    x_exp,
    exp_gain,
    routes,
    route_weight,
    w_gate,
    w_up,
    w_down,
):
    n, parts = lax.axis_size("ep"), lax.axis_size("tp")
    rows_a = x_mix.shape[0]
    rows_b, model = x_exp.shape
    head_size = query_gain.shape[0]
    width = w_query.shape[1]
    local = w_gate.shape[2]
    out_width = w_down.shape[2]
    head_count = width // (2 * head_size)
    top = routes.shape[1]
    cap = 3 * rows_b * top // (2 * n)
    cap = -(-cap // 16) * 16
    f32, bf16 = jnp.float32, jnp.bfloat16
    normed = rms_rows(x_mix, mix_gain, 1e-05).astype(bf16)

    def split_norm(weights, gain, scale):
        out = jnp.dot(normed, weights, preferred_element_type=f32)
        out = out.reshape(rows_a, head_count * 2, head_size)
        return (rms_rows(out, gain, 1e-06) * scale).astype(bf16).reshape(rows_a, width)

    queries = split_norm(w_query, query_gain, head_size ** (-0.5))
    key_rows = split_norm(w_key, key_gain, 1.0)
    values = jnp.dot(normed, w_value, preferred_element_type=f32).astype(bf16)
    both = jnp.concatenate([key_rows, values], axis=1)
    rows = rms_rows(x_exp, exp_gain, 1e-05).astype(bf16)
    info = jnp.concatenate([routes.astype(f32), route_weight], axis=1).T
    vmem = pl.BlockSpec(memory_space=pltpu.VMEM)
    smem = pl.BlockSpec(memory_space=pltpu.SMEM)
    dma = pltpu.SemaphoreType.DMA
    groups = 4
    return pl.pallas_call(
        functools.partial(kernel, n, parts, top, cap, head_size),
        out_shape=(
            jax.ShapeDtypeStruct((rows_a, w_mix_out.shape[1]), bf16),
            jax.ShapeDtypeStruct((rows_b, out_width), bf16),
        ),
        in_specs=[vmem, vmem, vmem, vmem, smem, vmem, vmem, vmem, vmem, vmem],
        out_specs=(vmem, vmem),
        scratch_shapes=[
            pltpu.VMEM((n, rows_a, 2 * width), bf16),
            pltpu.VMEM((n, rows_b, model), bf16),
            pltpu.VMEM((n, 2 * top, rows_b), f32),
            pltpu.VMEM((n * cap, model), bf16),
            pltpu.VMEM((parts, n * cap, local), bf16),
            pltpu.VMEM((n * cap, out_width), bf16),
            pltpu.VMEM((n, cap, out_width), bf16),
            pltpu.VMEM((2, rows_a, width), f32),
            pltpu.VMEM((2, head_count, rows_a, 128), f32),
            pltpu.VMEM((parts, rows_a, width), bf16),
            dma((n,)),
            dma((n,)),
            dma((n,)),
            dma((n,)),
            dma((n,)),
            dma((n,)),
            dma((n,)),
            dma((n,)),
            dma((groups * parts,)),
            dma((groups * parts,)),
            dma((n,)),
            dma((n,)),
            dma((parts,)),
            dma((parts,)),
        ],
        compiler_params=pltpu.CompilerParams(
            collective_id=0, has_side_effects=True, vmem_limit_bytes=60 * 1024 * 1024
        ),
    )(
        queries,
        both,
        rows,
        info,
        mix_lambda,
        head_gain.reshape(1, -1),
        w_mix_out,
        w_gate[0],
        w_up[0],
        w_down[0],
    )


def solution(mesh):
    return jax.shard_map(
        body,
        mesh=mesh,
        in_specs=(
            P("ep", None),
            P(),
            P(None, "tp"),
            P(None, "tp"),
            P(None, "tp"),
            P(),
            P(),
            P("tp"),
            P(),
            P(None, "tp"),
            P("ep", None),
            P(),
            P("ep", None),
            P("ep", None),
            P("ep", None, "tp"),
            P("ep", None, "tp"),
            P("ep", None, "tp"),
        ),
        out_specs=(P("ep", "tp"), P("ep", "tp")),
        check_vma=False,
    )
```

time: 234 us -> 126 us (0.54)
  the two profiles are of different devices: /device:TPU:0 before, /device:TPU:21 now
where the time goes in v1:
time: 126 us; the launch traced here: 125 us
  Pallas kernels  103 us (82%)
  other arithmetic  7.41 us (6%)
  matrix products  7.1 us (6%)
  local copies, waits for them, and re-layouts  6.54 us (5%)
    pallas_call x1, Pallas kernels, body(): pl.pallas_call(functools.partial(kernel, n, parts, top, cap, head_size),...  103 us
    dot_general x2, matrix products, split_norm(): out = jnp.dot(normed, weights, preferred_element_type=f32)  4.29 us
    unnamed x22, local copies, waits for them, and re-layouts  3.68 us
    convert_element_type x2, other arithmetic, split_norm(): (rms_rows(out, gain, 1e-06) * scale).astype(bf16).reshape(rows_a, width)  3.01 us
    dot_general x1, matrix products, body(): values = jnp.dot(normed, w_value, preferred_element_type=f32).astype(bf16)  2.81 us

profile of v1, /device:TPU:21, one launch (start us, length us, event | category | flops | bytes accessed | tf_op | source)
XLA Modules:
  0.0 125.3 jit_solution(463516621561493488)
XLA Ops:
  0.6 0.0 copy-start
  0.6 1.7 %fusion = f32[256]{0:T(256)S(1)} fusion(bf16[256,2048]{1,0:T(8,128)(2,1)} %param.17), kind=kLoop, calls=%fused_computation.2 | loop fusion | flops 1572608 | bytes 1049600 | tf_op jit(solution)/shard_map/reduce_sum | solution.py:12
  2.3 0.2 copy-done
  2.5 2.8 %fusion.11 = (f32[256,512]{1,0:T(8,128)S(1)}, f32[256,512]{1,0:T(8,128)}) fusion(bf16[2048,512]{1,0:T(8,128)(2,1)S(1)} %copy-done, bf16[256,2048]{1,0:T(8,128)(2,1)} %param.17, f32[2048]{0:T(1024)} %param.18, f32[256]{0:T(256)S(1)} %add_rsqrt_fusion.2), kind=kOutput, calls=%fused_computation.23 | convolution fusion | flops 539099136 | bytes 4203520 | tf_op jit(solution)/shard_map/dot_general | solution.py:377
  5.3 0.0 copy-start.6
  5.3 0.0 copy-start.9
  5.3 0.2 copy.19
  5.6 0.2 copy.20
  5.8 0.1 copy-done.6
  6.0 0.1 mul.116
  6.0 1.9 %multiply_convert_fusion.1.q_ref = bf16[256,512]{1,0:T(8,128)(2,1)} fusion(f32[256,512]{1,0:T(8,128)} %get-tuple-element.3, f32[256,512]{1,0:T(8,128)S(1)} %copy.20, f32[512]{0:T(512)S(1)} %mul.116), kind=kLoop, calls=%fused_computation.15 | loop fusion | flops 524288 | bytes 1312768 | tf_op jit(solution)/shard_map/convert_element_type | solution.py:379
  7.9 0.0 copy-done.9
  7.9 0.0 copy-start.2
  7.9 0.0 copy-start.8
  7.9 2.8 %convolution_convert_fusion = bf16[256,512]{1,0:T(8,128)(2,1)S(1)} fusion(bf16[2048,512]{1,0:T(8,128)(2,1)} %param.21, bf16[256,2048]{1,0:T(8,128)(2,1)} %param.17, f32[2048]{0:T(1024)S(1)} %copy-done.9, f32[256]{0:T(256)S(1)} %add_rsqrt_fusion.2), kind=kOutput, calls=%fused_computation.7 | convolution fusion | flops 539099136 | bytes 3417088 | tf_op jit(solution)/shard_map/dot_general | solution.py:383
  10.7 0.0 copy-done.2
  10.7 0.0 copy-done.8
  10.8 1.5 %fusion.12 = (f32[256,512]{1,0:T(8,128)S(1)}, f32[256,512]{1,0:T(8,128)}) fusion(bf16[2048,512]{1,0:T(8,128)(2,1)S(1)} %copy-done.8, bf16[256,2048]{1,0:T(8,128)(2,1)S(1)} %copy-done.2, f32[2048]{0:T(1024)S(1)} %copy-done.9, f32[256]{0:T(256)S(1)} %add_rsqrt_fusion.2), kind=kOutput, calls=%fused_computation.24 | convolution fusion | flops 539099136 | bytes 4203520 | tf_op jit(solution)/shard_map/dot_general | solution.py:377
  12.3 0.0 copy-start.7
  12.3 0.2 copy.21
  12.6 0.0 copy-start.1
  12.6 0.8 mul.123
  13.4 0.0 copy-start.3
  13.4 1.2 copy.22
  14.7 0.0 copy-done.7
  14.7 0.0 copy-start.4
  14.7 0.0 copy-start.5
  14.7 0.1 mul.127
  14.8 1.1 multiply_convert_fusion
  15.9 0.8 pad_maximum_fusion.kv_ref
  16.8 0.0 copy-done.1
  16.8 0.2 fusion.3
  17.0 0.0 copy-done.3
  17.0 1.0 fusion.5.tok_ref
  18.0 0.0 copy-done.4
  18.0 0.0 copy-done.5
  18.0 0.6 maximum_bitcast_fusion.info_ref
  18.6 103.4 %shard_map.176 = (bf16[256,512]{1,0:T(8,128)(2,1)}, bf16[128,512]{1,0:T(8,128)(2,1)}) custom-call(bf16[256,512]{1,0:T(8,128)(2,1)} %multiply_convert_fusion.1.q_ref, bf16[256,1024]{1,0:T(8,128)(2,1)} %pad_maximum_fusion.kv_ref, bf16[128,2048]{1,0:T(8,128)(2,1)} %fusion.5.tok_ref, f32[8,128]{1,0:T(8,128)} %maximum_bitcast_fusion.info_ref, f32[4]{0:T(128)} %lam_ref.1, ...), custom_call_target="tpu_custom_call" | custom-call | tf_op jit(solution)/shard_map/pallas_call | solution.py:391
  122.0 1.7 %copy.25 = bf16[256,512]{1,0:T(8,128)(2,1)} copy(bf16[256,512]{1,0:T(8,128)(2,1)} %get-tuple-element.8) | data formatting | bytes 524288
  123.7 1.6 %copy.26 = bf16[128,512]{1,0:T(8,128)(2,1)} copy(bf16[128,512]{1,0:T(8,128)(2,1)} %get-tuple-element.9) | data formatting | bytes 262144
  (10 shorter events, 0.2 us)
Async XLA Ops:
  0.6 1.9 %copy-start = (bf16[2048,512]{1,0:T(8,128)(2,1)S(1)}, bf16[2048,512]{1,0:T(8,128)(2,1)}, u32[]{:S(2)}) copy-start(bf16[2048,512]{1,0:T(8,128)(2,1)} %param.19) | copy-start | bytes 6291460
  5.3 0.7 copy-start.6
  5.3 2.6 %copy-start.9 = (f32[2048]{0:T(1024)S(1)}, f32[2048]{0:T(1024)}, u32[]{:S(2)}) copy-start(f32[2048]{0:T(1024)} %param.18) | copy-start | bytes 24580
  7.9 2.8 %copy-start.2 = (bf16[256,2048]{1,0:T(8,128)(2,1)S(1)}, bf16[256,2048]{1,0:T(8,128)(2,1)}, u32[]{:S(2)}) copy-start(bf16[256,2048]{1,0:T(8,128)(2,1)} %param.17) | copy-start | bytes 3145732
  7.9 2.9 %copy-start.8 = (bf16[2048,512]{1,0:T(8,128)(2,1)S(1)}, bf16[2048,512]{1,0:T(8,128)(2,1)}, u32[]{:S(2)}) copy-start(bf16[2048,512]{1,0:T(8,128)(2,1)} %param.20) | copy-start | bytes 6291460
  12.3 2.4 %copy-start.7 = (f32[64]{0:T(128)S(1)}, f32[64]{0:T(128)}, u32[]{:S(2)}) copy-start(f32[64]{0:T(128)} %param.23) | copy-start | bytes 772
  12.6 4.2 %copy-start.1 = (bf16[128,2048]{1,0:T(8,128)(2,1)S(1)}, bf16[128,2048]{1,0:T(8,128)(2,1)}, u32[]{:S(2)}) copy-start(bf16[128,2048]{1,0:T(8,128)(2,1)} %param.27) | copy-start | bytes 1572868
  13.4 3.6 %copy-start.3 = (f32[2048]{0:T(1024)S(1)}, f32[2048]{0:T(1024)}, u32[]{:S(2)}) copy-start(f32[2048]{0:T(1024)} %param.28) | copy-start | bytes 24580
  14.7 3.3 %copy-start.4 = (s32[128,4]{0,1:T(4,128)S(1)}, s32[128,4]{0,1:T(4,128)}, u32[]{:S(2)}) copy-start(s32[128,4]{0,1:T(4,128)} %param.29) | copy-start | bytes 6148
  14.7 3.3 %copy-start.5 = (f32[128,4]{0,1:T(4,128)S(1)}, f32[128,4]{0,1:T(4,128)}, u32[]{:S(2)}) copy-start(f32[128,4]{0,1:T(4,128)} %param.30) | copy-start | bytes 6148

commit v2 on v1

--- a/solution.py
+++ b/solution.py
@@ -18,18 +18,35 @@
     top,
     cap,
     head_size,
+    x_ref,
+    xgain_ref,
+    e_ref,
+    egain_ref,
+    gains_ref,
+    info_ref,
+    lam_ref,
+    hgain_ref,
+    wq_any,
+    wk_any,
+    wv_any,
+    wgate_any,
+    wup_any,
+    wdown_any,
+    wout_any,
+    attn_ref,
+    moe_ref,
+    wq_ref,
+    wk_ref,
+    wv_ref,
+    wgate_ref,
+    wup_ref,
+    wdown_ref,
+    wout_ref,
+    load_s,
+    normed,
     q_ref,
     kv_ref,
     tok_ref,
-    info_ref,
-    lam_ref,
-    hgain_ref,
-    wout_ref,
-    wgate_ref,
-    wup_ref,
-    wdown_ref,
-    attn_ref,
-    moe_ref,
     kv,
     tok,
     info,
@@ -76,6 +93,22 @@
     local = wgate_ref.shape[1]
     f32, bf16 = jnp.float32, jnp.bfloat16
 
+    loads = [
+        pltpu.make_async_copy(source, target, load_s.at[i])
+        for i, (source, target) in enumerate(
+            (
+                (wq_any, wq_ref),
+                (wk_any, wk_ref),
+                (wv_any, wv_ref),
+                (wgate_any.at[0], wgate_ref),
+                (wup_any.at[0], wup_ref),
+                (wdown_any.at[0], wdown_ref),
+                (wout_any, wout_ref),
+            )
+        )
+    ]
+    for load in loads:
+        load.start()
     barrier = pltpu.get_barrier_semaphore()
     for i in range(1, n):
         pl.semaphore_signal(
@@ -85,6 +118,7 @@
         pl.semaphore_signal(
             barrier, inc=1, device_id={"tp": (mine + i) % parts}, device_id_type=pl.DeviceIdType.MESH
         )
+    tok_ref[...] = rms_rows(e_ref[...], egain_ref[...], 1e-05).astype(bf16)
     pl.semaphore_wait(barrier, n - 1 + parts - 1)
 
     def push(src, dst, s_sem, r_sem, where):
@@ -105,42 +139,44 @@
     def held(step, way):
         return at(pos - step) if way == 0 else at(pos + step)
 
-    def tok_copies(step):
+    def tok_copies(step, piece):
         out = []
         for way in (0, 1):
             where = {"ep": right if way == 0 else left}
             b = held(step - 1, way)
-            cols = pl.ds(pl.multiple_of(core * side, side), side)
+            cols = pl.ds(pl.multiple_of(core * side + piece * (side // 2), side // 2), side // 2)
             rows = span(step, way, rows_b)
             if step == 1:
                 src = tok_ref.at[rows, cols]
             else:
                 src = tok.at[b, rows, cols]
             i = 2 * (step - 1) + way
-            out.append(push(src, tok.at[b, rows, cols], tok_s.at[i], tok_r.at[i], where))
-            if step < half or way == 0:
+            j = piece * n + i
+            out.append(push(src, tok.at[b, rows, cols], tok_s.at[j], tok_r.at[j], where))
+            if piece == 0 and (step < half or way == 0):
                 src = info_ref if step == 1 else info.at[b]
                 out.append(push(src, info.at[b], info_s.at[i], info_r.at[i], where))
         return out
 
-    def kv_copies(step):
+    def kv_copies(step, piece):
         out = []
         for way in (0, 1):
             where = {"ep": right if way == 0 else left}
             b = held(step - 1, way)
             rows = span(step, way, rows_a)
-            src = kv_ref.at[rows] if step == 1 else kv.at[b, rows]
-            i = 2 * (step - 1) + way
-            out.append(push(src, kv.at[b, rows], kv_s.at[i], kv_r.at[i], where))
+            cols = pl.ds(piece * width, width)
+            src = kv_ref.at[rows, cols] if step == 1 else kv.at[b, rows, cols]
+            i = 2 * (step - 1) + way + piece * n
+            out.append(push(src, kv.at[b, rows, cols], kv_s.at[i], kv_r.at[i], where))
         return out
 
-    def core_copies(step):
+    def core_copies(step, piece):
         out = []
         for way in (0, 1):
             b = held(step, way)
-            cols = pl.ds(pl.multiple_of(core * side, side), side)
+            cols = pl.ds(pl.multiple_of(core * side + piece * (side // 2), side // 2), side // 2)
             ref = tok.at[b, span(step, way, rows_b), cols]
-            i = 2 * (step - 1) + way
+            i = 2 * (step - 1) + way + piece * n
             out.append(push(ref, ref, core_s.at[i], core_r.at[i], {"tp": twin}))
         return out
 
@@ -198,11 +234,31 @@
             value = gate * jax.nn.sigmoid(1.702 * gate) * (up + 1.0)
             hid[mine, g * size : (g + 1) * size, cols] = value.astype(bf16)
 
+    def hid_ref(owner, g):
+        return hid.at[owner, pl.ds(g * size, size)]
+
+    def head_ref(owner, g):
+        return heads.at[owner]
+
+    def exchange(ref_of, g, sems):
         out = []
-        for i in range(1, parts):
-            ref = hid.at[mine, pl.ds(g * size, size)]
+        for i in range(0, parts, 2):
             k = g * parts + i
-            out.append(push(ref, ref, hid_s.at[k], hid_r.at[k], {"tp": (mine + i) % parts}))
+            ref = ref_of(mine, g)
+            if i == 0:
+                out.append(push(ref, ref, sems[0].at[k], sems[1].at[k], {"tp": twin}))
+            else:
+                where = {"tp": (mine + i) % parts}
+                out.append(push(ref, ref, sems[0].at[k], sems[1].at[k], where))
+        return start(out)
+
+    def relay(ref_of, g, sems, firsts):
+        out = []
+        for i in range(2, parts, 2):
+            firsts[i // 2].wait_recv()
+            k = g * parts + i + 1
+            ref = ref_of((mine + parts - i) % parts, g)
+            out.append(push(ref, ref, sems[0].at[k], sems[1].at[k], {"tp": twin}))
         return start(out)
 
     def attend(k_of, diagonal):
@@ -244,36 +300,79 @@
                 attend(lambda cols: kv[b, :, cols], False)
 
     sent = []
-    now = start(tok_copies(1))
-    sent += now
-    attend(lambda cols: kv_ref[:, cols], True)
-    cores, hids, kv_now = [], [], None
+    now = [start(tok_copies(1, piece)) for piece in (0, 1)]
+    sent += now[0] + now[1]
+    normed[...] = rms_rows(x_ref[...], xgain_ref[...], 1e-05).astype(bf16)
+    for load in loads[:3]:
+        load.wait()
+    wide = gains_ref.shape[1]
+
+    @pl.loop(0, width // wide)
+    def _(t):
+        cols = pl.ds(pl.multiple_of(t * wide, wide), wide)
+        vcols = pl.ds(pl.multiple_of(width + t * wide, wide), wide)
+        group = lax.broadcasted_iota(jnp.int32, (rows_a, wide), 1) // head_size
+
+        def unit(weights, gain):
+            out = jnp.dot(normed[...], weights[:, cols], preferred_element_type=f32)
+            square = out * out
+            factor = jnp.zeros_like(out)
+            for g in range(wide // head_size):
+                here = group == g
+                mean = jnp.sum(jnp.where(here, square, 0.0), axis=1, keepdims=True) / head_size
+                factor = jnp.where(here, lax.rsqrt(mean + 1e-06), factor)
+            return out * factor * gain
+
+        q_ref[:, cols] = (unit(wq_ref, gains_ref[0:1, :]) * head_size ** (-0.5)).astype(bf16)
+        kv_ref[:, cols] = unit(wk_ref, gains_ref[1:2, :]).astype(bf16)
+        kv_ref[:, vcols] = jnp.dot(
+            normed[...], wv_ref[:, cols], preferred_element_type=f32
+        ).astype(bf16)
+
+    for load in loads[3:5]:
+        load.wait()
+    hid_sems, head_sems = (hid_s, hid_r), (head_s, head_r)
+    hids, relays, kv_now = [], [], None
     early = max(1, half - 1)
     for step in range(1, half + 1):
-        wait_recv(now)
-        if step < half:
-            now = start(tok_copies(step + 1))
-            sent += now
+        cores, later = [], []
+        for piece in (0, 1):
+            wait_recv(now[piece])
+            if step < half:
+                later.append(start(tok_copies(step + 1, piece)))
+                sent += later[-1]
+            cores += start(core_copies(step, piece))
+        sent += cores
+        now = later
         if step == early:
-            kv_now = start(kv_copies(1))
-            sent += kv_now
-        cores = start(core_copies(step))
-        sent += cores
+            kv_now = [start(kv_copies(1, piece)) for piece in (0, 1)]
+            sent += kv_now[0] + kv_now[1]
+        if step == 1:
+            attend(lambda cols: kv_ref[:, cols], True)
+        if hids:
+            relays += relay(hid_ref, len(hids) - 1, hid_sems, hids[-1])
         wait_recv(cores)
         for g in range(groups):
             if (g * per + per) // 2 == step:
-                hids += hidden_group(g)
-    sent += hids
+                hidden_group(g)
+                hids.append(exchange(hid_ref, g, hid_sems))
 
     moe_step = (half + 1) // 2
     for step in range(1, half + 1):
-        wait_recv(kv_now)
-        if step < half:
-            kv_now = start(kv_copies(step + 1))
-            sent += kv_now
-        attend_step(step)
+        later = []
+        for piece in (0, 1):
+            wait_recv(kv_now[piece])
+            if step < half:
+                later.append(start(kv_copies(step + 1, piece)))
+                sent += later[-1]
+        kv_now = later
+        if step == 1:
+            relays += relay(hid_ref, groups - 1, hid_sems, hids[-1])
         if step == moe_step:
-            wait_recv(hids)
+            loads[5].wait()
+            for copies in hids:
+                copies[0].wait_recv()
+            wait_recv(relays)
 
             @pl.loop(0, groups)
             def _(g):
@@ -302,6 +401,7 @@
                     )
                 )
             sent += start(rets)
+        attend_step(step)
 
     @pl.loop(0, width // (2 * head_size))
     def _(h):
@@ -311,11 +411,11 @@
         mix = first - lam_ref[h] * second
         heads[mine, :, cols] = (rms_rows(mix, hgain_ref[...], 1e-05) * 0.8).astype(bf16)
 
-    outs = []
-    for i in range(1, parts):
-        ref = heads.at[mine]
-        outs.append(push(ref, ref, head_s.at[i], head_r.at[i], {"tp": (mine + i) % parts}))
-    sent += start(outs)
+    outs = exchange(head_ref, 0, head_sems)
+    passed = relay(head_ref, 0, head_sems, outs)
+    for copies in hids:
+        sent += copies
+    sent += relays + outs + passed
 
     wait_recv(rets)
     total = jnp.zeros(moe_ref.shape, f32)
@@ -329,7 +429,9 @@
         total += picked * weight.T
     moe_ref[...] = total.astype(bf16)
 
-    wait_recv(outs)
+    loads[6].wait()
+    outs[0].wait_recv()
+    wait_recv(passed)
     result = jnp.zeros(attn_ref.shape, f32)
     for t in range(parts):
         result += jnp.dot(
@@ -371,21 +473,12 @@
     cap = 3 * rows_b * top // (2 * n)
     cap = -(-cap // 16) * 16
     f32, bf16 = jnp.float32, jnp.bfloat16
-    normed = rms_rows(x_mix, mix_gain, 1e-05).astype(bf16)
-
-    def split_norm(weights, gain, scale):
-        out = jnp.dot(normed, weights, preferred_element_type=f32)
-        out = out.reshape(rows_a, head_count * 2, head_size)
-        return (rms_rows(out, gain, 1e-06) * scale).astype(bf16).reshape(rows_a, width)
-
-    queries = split_norm(w_query, query_gain, head_size ** (-0.5))
-    key_rows = split_norm(w_key, key_gain, 1.0)
-    values = jnp.dot(normed, w_value, preferred_element_type=f32).astype(bf16)
-    both = jnp.concatenate([key_rows, values], axis=1)
-    rows = rms_rows(x_exp, exp_gain, 1e-05).astype(bf16)
+    wide = min(256, width)
+    gains = jnp.tile(jnp.stack([query_gain, key_gain]), (1, wide // head_size))
     info = jnp.concatenate([routes.astype(f32), route_weight], axis=1).T
     vmem = pl.BlockSpec(memory_space=pltpu.VMEM)
     smem = pl.BlockSpec(memory_space=pltpu.SMEM)
+    hbm = pl.BlockSpec(memory_space=pl.ANY)
     dma = pltpu.SemaphoreType.DMA
     groups = 4
     return pl.pallas_call(
@@ -394,9 +487,21 @@
             jax.ShapeDtypeStruct((rows_a, w_mix_out.shape[1]), bf16),
             jax.ShapeDtypeStruct((rows_b, out_width), bf16),
         ),
-        in_specs=[vmem, vmem, vmem, vmem, smem, vmem, vmem, vmem, vmem, vmem],
+        in_specs=[vmem] * 6 + [smem, vmem] + [hbm] * 7,
         out_specs=(vmem, vmem),
         scratch_shapes=[
+            pltpu.VMEM(w_query.shape, bf16),
+            pltpu.VMEM(w_key.shape, bf16),
+            pltpu.VMEM(w_value.shape, bf16),
+            pltpu.VMEM(w_gate.shape[1:], bf16),
+            pltpu.VMEM(w_up.shape[1:], bf16),
+            pltpu.VMEM(w_down.shape[1:], bf16),
+            pltpu.VMEM(w_mix_out.shape, bf16),
+            dma((7,)),
+            pltpu.VMEM((rows_a, model), bf16),
+            pltpu.VMEM((rows_a, width), bf16),
+            pltpu.VMEM((rows_a, 2 * width), bf16),
+            pltpu.VMEM((rows_b, model), bf16),
             pltpu.VMEM((n, rows_a, 2 * width), bf16),
             pltpu.VMEM((n, rows_b, model), bf16),
             pltpu.VMEM((n, 2 * top, rows_b), f32),
@@ -407,14 +512,14 @@
             pltpu.VMEM((2, rows_a, width), f32),
             pltpu.VMEM((2, head_count, rows_a, 128), f32),
             pltpu.VMEM((parts, rows_a, width), bf16),
+            dma((2 * n,)),
+            dma((2 * n,)),
             dma((n,)),
             dma((n,)),
-            dma((n,)),
-            dma((n,)),
-            dma((n,)),
-            dma((n,)),
-            dma((n,)),
-            dma((n,)),
+            dma((2 * n,)),
+            dma((2 * n,)),
+            dma((2 * n,)),
+            dma((2 * n,)),
             dma((groups * parts,)),
             dma((groups * parts,)),
             dma((n,)),
@@ -426,16 +531,21 @@
             collective_id=0, has_side_effects=True, vmem_limit_bytes=60 * 1024 * 1024
         ),
     )(
-        queries,
-        both,
-        rows,
+        x_mix,
+        mix_gain.reshape(1, -1),
+        x_exp,
+        exp_gain.reshape(1, -1),
+        gains,
         info,
         mix_lambda,
         head_gain.reshape(1, -1),
+        w_query,
+        w_key,
+        w_value,
+        w_gate,
+        w_up,
+        w_down,
         w_mix_out,
-        w_gate[0],
-        w_up[0],
-        w_down[0],
     )
 
 

time: 126 us -> 106 us (0.84)
  matrix products: 7.1 us -> 0 us
  Pallas kernels: 103 us -> 97.8 us
  other arithmetic: 7.41 us -> 2.64 us
  local copies, waits for them, and re-layouts: 6.54 us -> 3.9 us
    dot_general x3 -> x0, matrix products: 7.1 us -> none  [the longest x2 4.29 us: split_norm(): out = jnp.dot(normed, weights, preferred_element_type=f32)]
    pallas_call x1, Pallas kernels: 103 us -> 97.8 us  [body(): pl.pallas_call(functools.partial(kernel, n, parts, top, cap, head_size),...]
    convert_element_type x3 -> x0, other arithmetic: 3.99 us -> none  [the longest x2 3.01 us: split_norm(): (rms_rows(out, gain, 1e-06) * scale).astype(bf16).reshape(rows_a, width)]
    mul x10 -> x0, local copies, waits for them, and re-layouts: 2.86 us -> none  [the longest x8 2.47 us: rms_rows(): wide * lax.rsqrt(jnp.mean(wide * wide, axis=-1, keepdims=True) + epsilon)]
    reduce_sum x4 -> x0, other arithmetic: 1.94 us -> none  [rms_rows(): jnp.mean(wide * wide, axis=-1, keepdims=True) + epsilon]
    unnamed x22 -> x2, local copies, waits for them, and re-layouts: 3.68 us -> 3.24 us
where the time goes in v2:
time: 106 us; the launch traced here: 105 us
  Pallas kernels  97.8 us (92%)
  local copies, waits for them, and re-layouts  3.9 us (4%)
  other arithmetic  2.64 us (2%)
    pallas_call x1, Pallas kernels, body(): pl.pallas_call(functools.partial(kernel, n, parts, top, cap, head_size),...  97.8 us
    unnamed x2, local copies, waits for them, and re-layouts  3.24 us

profile of v2, /device:TPU:21, one launch (start us, length us, event | category | flops | bytes accessed | tf_op | source)
XLA Modules:
  0.0 105.0 jit_solution(16801171568138980965)
XLA Ops:
  0.6 0.7 pad_maximum_fusion
  1.3 0.7 convert_element_type.3
  2.0 1.3 %maximum_bitcast_fusion.info_ref = f32[8,128]{1,0:T(8,128)} fusion(f32[128,4]{0,1:T(4,128)} %param.30, f32[128,4]{0,1:T(4,128)S(1)} %convert_element_type.3), kind=kLoop, calls=%fused_computation | loop fusion | flops 1024 | bytes 8192 | tf_op jit(solution)/shard_map/transpose | solution.py:478
  3.3 0.7 tile.10.gains_ref
  3.9 97.8 %shard_map.176 = (bf16[256,512]{1,0:T(8,128)(2,1)}, bf16[128,512]{1,0:T(8,128)(2,1)}) custom-call(bf16[256,2048]{1,0:T(8,128)(2,1)} %x_ref.1, f32[1,2048]{1,0:T(1,128)} %bitcast.7, bf16[128,2048]{1,0:T(8,128)(2,1)} %e_ref.1, f32[1,2048]{1,0:T(1,128)} %bitcast.8, f32[2,256]{1,0:T(2,128)} %tile.10.gains_ref, f32[8,128]{1,0:T(8,128)} %maximum_bitcast_fusion.info_ref, ...), custom_call_target="tpu_custom_call" | custom-call | tf_op jit(solution)/shard_map/pallas_call | solution.py:484
  101.8 1.7 %copy.21 = bf16[256,512]{1,0:T(8,128)(2,1)} copy(bf16[256,512]{1,0:T(8,128)(2,1)} %get-tuple-element.4) | data formatting | bytes 524288
  103.4 1.6 %copy.22 = bf16[128,512]{1,0:T(8,128)(2,1)} copy(bf16[128,512]{1,0:T(8,128)(2,1)} %get-tuple-element.5) | data formatting | bytes 262144
  (1 shorter events, 0.0 us)

commit v3 on v2

--- a/solution.py
+++ b/solution.py
@@ -333,7 +333,7 @@
         load.wait()
     hid_sems, head_sems = (hid_s, hid_r), (head_s, head_r)
     hids, relays, kv_now = [], [], None
-    early = max(1, half - 1)
+    early = max(1, half - 2)
     for step in range(1, half + 1):
         cores, later = [], []
         for piece in (0, 1):

time: 106 us -> 111 us (1.047)
  Pallas kernels: 97.8 us -> 102 us
    pallas_call x1, Pallas kernels: 97.8 us -> 102 us  [body(): pl.pallas_call(functools.partial(kernel, n, parts, top, cap, head_size),...]
where the time goes in v3:
time: 111 us; the launch traced here: 110 us
  Pallas kernels  102 us (92%)
  local copies, waits for them, and re-layouts  3.9 us (4%)
  other arithmetic  2.64 us (2%)
    pallas_call x1, Pallas kernels, body(): pl.pallas_call(functools.partial(kernel, n, parts, top, cap, head_size),...  102 us
    unnamed x2, local copies, waits for them, and re-layouts  3.24 us

profile of v3, /device:TPU:21, one launch (start us, length us, event | category | flops | bytes accessed | tf_op | source)
XLA Modules:
  0.0 109.6 jit_solution(16710660165058579109)
XLA Ops:
  0.6 0.7 pad_maximum_fusion
  1.3 0.7 convert_element_type.3
  2.0 1.3 %maximum_bitcast_fusion.info_ref = f32[8,128]{1,0:T(8,128)} fusion(f32[128,4]{0,1:T(4,128)} %param.30, f32[128,4]{0,1:T(4,128)S(1)} %convert_element_type.3), kind=kLoop, calls=%fused_computation | loop fusion | flops 1024 | bytes 8192 | tf_op jit(solution)/shard_map/transpose | solution.py:478
  3.3 0.7 tile.10.gains_ref
  3.9 102.4 %shard_map.176 = (bf16[256,512]{1,0:T(8,128)(2,1)}, bf16[128,512]{1,0:T(8,128)(2,1)}) custom-call(bf16[256,2048]{1,0:T(8,128)(2,1)} %x_ref.1, f32[1,2048]{1,0:T(1,128)} %bitcast.7, bf16[128,2048]{1,0:T(8,128)(2,1)} %e_ref.1, f32[1,2048]{1,0:T(1,128)} %bitcast.8, f32[2,256]{1,0:T(2,128)} %tile.10.gains_ref, f32[8,128]{1,0:T(8,128)} %maximum_bitcast_fusion.info_ref, ...), custom_call_target="tpu_custom_call" | custom-call | tf_op jit(solution)/shard_map/pallas_call | solution.py:484
  106.4 1.7 %copy.21 = bf16[256,512]{1,0:T(8,128)(2,1)} copy(bf16[256,512]{1,0:T(8,128)(2,1)} %get-tuple-element.4) | data formatting | bytes 524288
  108.0 1.6 %copy.22 = bf16[128,512]{1,0:T(8,128)(2,1)} copy(bf16[128,512]{1,0:T(8,128)(2,1)} %get-tuple-element.5) | data formatting | bytes 262144
  (1 shorter events, 0.0 us)
